TPU v7x, 32 devices: a whole 2x2x4 slice. The times are simulated.
32 devices in a mesh: ep: 4 (over y, x), tp: 8 (over z, core).
Axes of the slice: x: 2, y: 2, z: 4, core: 2. Of those that a mesh axis runs over, the one named last changes fastest.
Arguments:
- tokens: bfloat16 [128, 2048], P('ep', 'tp'), may hold values from -80 to 80
- delta_state: float32 [128, 16, 128, 128], P('ep', 'tp'), may hold values from -1.8 to 1.8
- mix_gain: bfloat16 [2048], replicated, may hold values from 0.099609375 to 1.8984375
- w_query: bfloat16 [2048, 2048], P(None, 'tp'), may hold values from -0.125 to 0.125
- w_key: bfloat16 [2048, 2048], P(None, 'tp'), may hold values from -0.125 to 0.125
- w_value: bfloat16 [2048, 2048], P(None, 'tp'), may hold values from -0.125 to 0.125
- w_outgate: bfloat16 [2048, 2048], P(None, 'tp'), may hold values from -0.125 to 0.125
- w_beta: bfloat16 [2048, 16], P(None, 'tp'), may hold values from -0.125 to 0.125
- w_decay: bfloat16 [2048, 16], P(None, 'tp'), may hold values from -0.125 to 0.125
- decay_scale: float32 [16], P('tp'), may hold values from 0.05 to 1.5
- decay_bias: float32 [16], P('tp'), may hold values from -1.5 to 1.5
- head_gain: bfloat16 [128], replicated, may hold values from 0.099609375 to 1.8984375
- w_output: bfloat16 [2048, 2048], P('tp'), may hold values from -0.125 to 0.125
- ffn_gain: bfloat16 [2048], replicated, may hold values from 0.099609375 to 1.8984375
- route_ids: int32 [128, 6], P('ep'), may hold values from 0 to 31, all different within a row; in each aligned block of 32 rows (0 to 31, 32 to 63, ...) at most 16 rows name the same one
- route_weights: float32 [128, 6], P('ep'), may hold values from 0.2 to 1.2
- expert_gate: bfloat16 [32, 2048, 512], P(('ep', 'tp')), may hold values from -0.125 to 0.125
- expert_up: bfloat16 [32, 2048, 512], P(('ep', 'tp')), may hold values from -0.125 to 0.125
- expert_down: bfloat16 [32, 512, 2048], P(('ep', 'tp')), may hold values from -0.25 to 0.25
- shared_gate: bfloat16 [2048, 512], P(None, 'tp'), may hold values from -0.125 to 0.125
- shared_up: bfloat16 [2048, 512], P(None, 'tp'), may hold values from -0.125 to 0.125
- shared_down: bfloat16 [512, 2048], P('tp'), may hold values from -0.25 to 0.25
Outputs:
- layer_out: bfloat16 [128, 2048], P('ep', 'tp')
- new_state: float32 [128, 16, 128, 128], P('ep', 'tp')
Inputs may be any that keep to these rules, and one draw needn't show every extreme that they name: `route_ids`: each row names 6 different experts. In each aligned block of 32 rows (the sequences of one index of ep) no expert is named by more than 16 rows, and in every draw some expert is named by exactly 16 rows of some block.
All inputs are finite; a program needn't handle non-finite values.
Results may differ from a plain program's by a relative error of at most 0.013.
Values may be sent and summed in bfloat16 or wider, within the bound.
No kernel may reach another device: no remote copies, remote signals or barrier semaphores. Data moves between devices by JAX's collectives and lax.ppermute only.
A program may use at most 64 MiB of HBM per device.

v0:
```python
import jax
import jax.numpy as jnp
from jax import lax
from jax.sharding import PartitionSpec as P

epsilon = 1e-06


def rms_norm(values, gain_vector):
    squares = jnp.mean(values * values, axis=-1, keepdims=True)
    return values * lax.rsqrt(squares + epsilon) * gain_vector.astype(jnp.float32)


def unit_rows(values):
    return values * lax.rsqrt(jnp.sum(values * values, axis=-1, keepdims=True) + epsilon)


def expert_block(rows, expert_gate, expert_up, expert_down):
    gate_part = jnp.einsum("sjnd,jdf->sjnf", rows, expert_gate, preferred_element_type=jnp.float32)
    up_part = jnp.einsum("sjnd,jdf->sjnf", rows, expert_up, preferred_element_type=jnp.float32)
    hidden = (jax.nn.silu(gate_part) * up_part).astype(jnp.bfloat16)
    outputs = jnp.einsum("sjnf,jfd->sjnd", hidden, expert_down, preferred_element_type=jnp.float32)
    return outputs.astype(jnp.bfloat16)


def body(
    tokens,
    delta_state,
    mix_gain,
    w_query,
    w_key,
    w_value,
    w_outgate,
    w_beta,
    w_decay,
    decay_scale,
    decay_bias,
    head_gain,
    w_output,
    ffn_gain,
    route_ids,
    route_weights,
    expert_gate,
    expert_up,
    expert_down,
    shared_gate,
    shared_up,
    shared_down,
):
    rows_count = tokens.shape[0]
    width_own = tokens.shape[1]
    heads_here = delta_state.shape[1]
    key_size = delta_state.shape[2]
    tp_index = lax.axis_index("tp")
    full_rows = lax.all_gather(tokens, "tp", axis=1, tiled=True)
    resid_in = full_rows.astype(jnp.float32)
    normed_mix = rms_norm(resid_in, mix_gain).astype(jnp.bfloat16)

    def project(weight):
        result = jnp.dot(normed_mix, weight, preferred_element_type=jnp.float32)
        result = lax.optimization_barrier(result.astype(jnp.bfloat16)).astype(jnp.float32)
        return result.reshape(rows_count, heads_here, -1)

    query_unit = unit_rows(project(w_query)) * key_size ** (-0.5)
    key_unit = unit_rows(project(w_key))
    values_new = project(w_value)
    out_gate = project(w_outgate)
    beta_gate = jax.nn.sigmoid(jnp.dot(normed_mix, w_beta, preferred_element_type=jnp.float32))
    decay_input = jnp.dot(normed_mix, w_decay, preferred_element_type=jnp.float32) + decay_bias
    decay_rate = jnp.exp(-decay_scale * jax.nn.softplus(decay_input))
    key_read = jnp.einsum("shk,shkv->shv", key_unit, delta_state)
    written = beta_gate[:, :, None] * key_unit
    kept_state = delta_state - written[:, :, :, None] * key_read[:, :, None, :]
    new_state = (
        decay_rate[:, :, None, None] * kept_state
        + written[:, :, :, None] * values_new[:, :, None, :]
    )
    state_read = jnp.einsum("shk,shkv->shv", query_unit, new_state)
    gated = (
        (rms_norm(state_read, head_gain) * jax.nn.silu(out_gate))
        .reshape(rows_count, -1)
        .astype(jnp.bfloat16)
    )
    partial_value = jnp.dot(gated, w_output, preferred_element_type=jnp.float32)
    mixed_rows = lax.psum(partial_value.astype(jnp.bfloat16), "tp").astype(jnp.float32)
    resid_mid = resid_in + mixed_rows
    normed_ffn = rms_norm(resid_mid, ffn_gain).astype(jnp.bfloat16)
    resid_own = lax.dynamic_slice_in_dim(resid_mid, tp_index * width_own, width_own, 1)
    model_width = normed_ffn.shape[1]
    ep_count = lax.axis_size("ep")
    tp_count = lax.axis_size("tp")
    experts_here = expert_gate.shape[0]
    top_count = route_ids.shape[1]
    expert_total = experts_here * ep_count * tp_count
    capacity = max(2, 8 * rows_count * top_count // (3 * expert_total))
    pair_count = rows_count * top_count
    flat_ids = route_ids.reshape(pair_count)
    owner_ep = flat_ids // (tp_count * experts_here)
    owner_tp = flat_ids // experts_here % tp_count
    local_slot = flat_ids % experts_here
    mine_mask = owner_tp == tp_index
    pair_weights = jnp.where(mine_mask, route_weights.reshape(pair_count), 0.0)
    pair_index = jnp.arange(pair_count, dtype=jnp.int32)
    earlier = (flat_ids[:, None] == flat_ids[None, :]) & (pair_index[None, :] < pair_index[:, None])
    slot_rank = jnp.sum(earlier.astype(jnp.int32), axis=1)
    slot_count = ep_count * experts_here * capacity
    target = jnp.where(mine_mask, (owner_ep * experts_here + local_slot) * capacity + slot_rank, -1)
    choose = (target[:, None] == jnp.arange(slot_count, dtype=jnp.int32)[None, :]).astype(
        jnp.bfloat16
    )
    by_row = jnp.sum(choose.reshape(rows_count, top_count, slot_count), axis=1)
    outgoing = jnp.einsum("sb,sd->bd", by_row, normed_ffn, preferred_element_type=jnp.float32)
    outgoing = outgoing.astype(jnp.bfloat16).reshape(ep_count, experts_here, capacity, model_width)
    results = expert_block(
        lax.all_to_all(outgoing, "ep", split_axis=0, concat_axis=0, tiled=True),
        expert_gate,
        expert_up,
        expert_down,
    )
    returned = lax.all_to_all(results, "ep", split_axis=0, concat_axis=0, tiled=True)
    picked = jnp.dot(
        choose, returned.reshape(slot_count, model_width), preferred_element_type=jnp.float32
    )
    routed = jnp.sum(
        (pair_weights[:, None] * picked).reshape(rows_count, top_count, model_width), axis=1
    )
    shared_gate_part = jnp.dot(normed_ffn, shared_gate, preferred_element_type=jnp.float32)
    shared_up_part = jnp.dot(normed_ffn, shared_up, preferred_element_type=jnp.float32)
    hidden_shared = (jax.nn.silu(shared_gate_part) * shared_up_part).astype(jnp.bfloat16)
    branch_sum = routed + jnp.dot(hidden_shared, shared_down, preferred_element_type=jnp.float32)
    combined = lax.psum_scatter(
        branch_sum.astype(jnp.bfloat16), "tp", scatter_dimension=1, tiled=True
    ).astype(jnp.float32)
    layer_out = (resid_own + combined).astype(jnp.bfloat16)
    return (layer_out, new_state)


def solution(mesh):
    return jax.shard_map(
        body,
        mesh=mesh,
        in_specs=(
            P("ep", "tp"),
            P("ep", "tp", None, None),
            P(),
            P(None, "tp"),
            P(None, "tp"),
            P(None, "tp"),
            P(None, "tp"),
            P(None, "tp"),
            P(None, "tp"),
            P("tp"),
            P("tp"),
            P(),
            P("tp", None),
            P(),
            P("ep", None),
            P("ep", None),
            P(("ep", "tp"), None, None),
            P(("ep", "tp"), None, None),
            P(("ep", "tp"), None, None),
            P(None, "tp"),
            P(None, "tp"),
            P("tp", None),
        ),
        out_specs=(P("ep", "tp"), P("ep", "tp", None, None)),
        check_vma=False,
    )
```

profile of v0, /device:TPU:0, one launch (start us, length us, event | category | flops | bytes accessed | tf_op | source)
XLA Modules:
  0.0 168.9 jit_solution(10965425534985928686)
XLA Ops:
  7.2 0.0 copy-start
  7.2 0.0 all-reduce.2.cloned.1.call-start
  7.2 16.1 %all_gather.3 = bf16[32,2048]{1,0:T(8,128)(2,1)S(1)} all-gather(bf16[32,256]{1,0:T(8,128)(2,1)} %param.22), channel_id=1, replica_groups=mesh['ep'=4,'tp'=8] {'tp'}, dimensions={1}, use_global_device_ids=true | all-gather | bytes 147456 | tf_op jit(solution)/shard_map/all_gather | solution.py:55
  23.3 0.1 fusion.28
  23.5 0.7 convert_element_type.86
  24.1 1.5 convolution_convert_fusion.5
  25.7 0.1 multiply_reduce_fusion.2
  25.9 0.9 fusion.25
  26.8 0.1 copy.46
  26.9 1.6 convolution_convert_fusion.4
  28.5 0.7 neg.22
  29.1 0.9 fusion.61
  30.1 0.1 copy.45
  30.1 1.6 convolution_convert_fusion.6
  31.7 0.0 copy-start.1
  31.8 0.1 multiply_reduce_fusion.3
  31.9 0.1 multiply_multiply_fusion
  32.0 0.1 broadcast_multiply_fusion.1
  32.1 3.0 %fusion.72 = f32[32,2,1,128]{3,2,1,0:T(1,128)S(1)} fusion(f32[32,2,128,1]{2,3,1,0:T(1,128)S(1)} %bitcast.104, f32[32,2,128,128]{3,2,1,0:T(8,128)} %param.23), kind=kOutput, calls=%fused_computation.103 | convolution fusion | flops 2097152 | bytes 4259840 | tf_op jit(solution)/shard_map/shk,shkv->shv/dot_general | solution.py:71
  35.2 0.0 copy-done.1
  35.2 1.5 multiply_add_fusion
  36.7 0.0 copy-start.2
  36.8 0.0 copy-start.4
  36.8 0.0 copy-start.10
  36.8 0.0 copy-start.3
  36.8 0.0 copy-start.7
  36.8 0.0 copy-start.8
  36.8 0.0 copy-start.9
  36.8 2.1 %copy-done.2 = f32[32,2,128,128]{3,2,1,0:T(8,128)} copy-done((f32[32,2,128,128]{3,2,1,0:T(8,128)}, f32[32,2,128,128]{3,2,1,0:T(8,128)S(1)}, u32[]{:S(2)}) %copy-start.2) | copy-done | bytes 4194328
  38.9 0.6 fusion.73
  39.5 0.1 multiply_reduce_fusion.1
  39.7 0.0 copy-done.4
  39.7 0.3 convolution_convert_fusion.3
  40.1 0.1 fusion.45
  40.2 0.9 convolution_convert_fusion.2
  41.1 0.0 all-reduce.2.cloned.1.call-update
  41.2 0.1 copy.47
  41.3 0.1 reshape.196
  41.4 0.2 convert_reduce_fusion
  41.6 0.1 reduce_sum.82
  41.7 0.1 copy.53
  41.8 0.1 copy.48
  41.9 0.1 reshape.197
  42.0 0.1 fusion.42
  42.1 55.1 %all-reduce.2.cloned.1.call-done = bf16[32,2048]{1,0:T(8,128)(2,1)} async-done(((bf16[32,2048]{1,0:T(8,128)(2,1)}), bf16[32,2048]{1,0:T(8,128)(2,1)}) %all-reduce.2.cloned.1.call-update) | async-done | bytes 131088 | tf_op jit(solution)/shard_map/psum | solution.py:85
  97.3 1.1 convert_add_fusion
  98.3 1.0 multiply_convert_fusion
  99.3 0.9 convolution_convert_fusion.1
  100.3 3.8 %all-to-all-start = ((bf16[4,1,16,2048]{3,2,1,0:T(8,128)(2,1)}), bf16[4,1,16,2048]{3,2,1,0:T(8,128)(2,1)S(1)}, u32[]{:S(2)}, u32[]{:S(2)}) async-start(bf16[4,1,16,2048]{3,2,1,0:T(8,128)(2,1)} %bitcast.9), calls=%async_computation | async-start | bytes 524288 | tf_op jit(solution)/shard_map/all_to_all | solution.py:115
  104.1 5.4 %all-to-all-done = bf16[4,1,16,2048]{3,2,1,0:T(8,128)(2,1)S(1)} async-done(((bf16[4,1,16,2048]{3,2,1,0:T(8,128)(2,1)}), bf16[4,1,16,2048]{3,2,1,0:T(8,128)(2,1)S(1)}, u32[]{:S(2)}, u32[]{:S(2)}) %all-to-all-start) | async-done | bytes 262176 | tf_op jit(solution)/shard_map/all_to_all | solution.py:115
  109.4 2.1 %fusion.7 = f32[4,1,16,512]{3,2,0,1:T(8,128)S(1)} fusion(bf16[1,2048,512]{2,1,0:T(8,128)(2,1)} %param.38, bf16[4,1,16,2048]{3,2,1,0:T(8,128)(2,1)S(1)} %all-to-all-done), kind=kOutput, calls=%fused_computation.13 | convolution fusion | flops 134217728 | bytes 2490368 | tf_op jit(solution)/shard_map/sjnd,jdf->sjnf/dot_general | solution.py:19
  111.5 3.2 %fusion = bf16[4,1,16,2048]{3,2,1,0:T(8,128)(2,1)} fusion(bf16[1,512,2048]{2,1,0:T(8,128)(2,1)S(1)} %copy-done, bf16[1,2048,512]{2,1,0:T(8,128)(2,1)} %param.39, bf16[4,1,16,2048]{3,2,1,0:T(8,128)(2,1)S(1)} %all-to-all-done, f32[4,1,16,512]{3,2,0,1:T(8,128)S(1)} %fusion.7), kind=kOutput, calls=%fused_computation.4 | convolution fusion | flops 268763136 | bytes 4849664 | tf_op jit(solution)/shard_map/sjnf,jfd->sjnd/dot_general | solution.py:22
  114.7 3.4 %all-to-all-start.1 = ((bf16[4,1,16,2048]{3,2,1,0:T(8,128)(2,1)}), bf16[4,1,16,2048]{3,2,1,0:T(8,128)(2,1)S(1)}, u32[]{:S(2)}, u32[]{:S(2)}) async-start(bf16[4,1,16,2048]{3,2,1,0:T(8,128)(2,1)} %fusion), calls=%async_computation.1 | async-start | bytes 524288 | tf_op jit(solution)/shard_map/all_to_all | solution.py:120
  118.1 0.0 copy-start.6
  118.1 0.0 reduce-scatter.2.cloned.1.call-start
  118.2 0.2 fusion.74
  118.4 5.1 %all-to-all-done.1 = bf16[4,1,16,2048]{3,2,1,0:T(8,128)(2,1)S(1)} async-done(((bf16[4,1,16,2048]{3,2,1,0:T(8,128)(2,1)}), bf16[4,1,16,2048]{3,2,1,0:T(8,128)(2,1)S(1)}, u32[]{:S(2)}, u32[]{:S(2)}) %all-to-all-start.1) | async-done | bytes 262176 | tf_op jit(solution)/shard_map/all_to_all | solution.py:120
  123.5 1.6 convolution_multiply_fusion
  125.0 2.7 %reshape.205 = f32[32,6,2048]{2,1,0:T(8,128)} reshape(f32[192,2048]{1,0:T(8,128)} %convolution_multiply_fusion) | data formatting | bytes 3145728 | tf_op jit(solution)/shard_map/reshape | solution.py:125
  127.7 2.2 %reduce_sum.85 = f32[32,2048]{1,0:T(8,128)S(1)} reduce(f32[32,6,2048]{2,1,0:T(8,128)} %reshape.205, f32[]{:T(128)} %constant.67.clone.1), dimensions={1}, to_apply=%region_8.9 | reduce | flops 327680 | bytes 1835012 | tf_op jit(solution)/shard_map/reduce_sum | solution.py:124
  130.0 2.0 %fusion.1 = bf16[32,2048]{1,0:T(8,128)(2,1)} fusion(f32[32,2048]{1,0:T(8,128)S(1)} %reduce_sum.85, bf16[64,2048]{1,0:T(8,128)(2,1)S(1)} %copy-done.6, bf16[32,2048]{1,0:T(8,128)(2,1)S(1)} %multiply_convert_fusion, bf16[2048,64]{0,1:T(8,128)(2,1)} %param.42, f32[32,64]{1,0:T(8,128)S(1)} %fusion.74), kind=kOutput, calls=%fused_computation.6 | convolution fusion | flops 16920576 | bytes 1056768 | tf_op jit(solution)/shard_map/dot_general | solution.py:130
  132.0 0.0 reduce-scatter.2.cloned.1.call-update
  132.0 28.7 %reduce-scatter.2.cloned.1.call-done = bf16[32,256]{1,0:T(8,128)(2,1)} async-done(((bf16[32,2048]{1,0:T(8,128)(2,1)}), bf16[32,256]{1,0:T(8,128)(2,1)}) %reduce-scatter.2.cloned.1.call-update) | async-done | bytes 16400 | tf_op jit(solution)/shard_map/reduce_scatter | solution.py:131
  160.7 1.3 add_convert_fusion
  (23 shorter events, 0.2 us)
Async XLA Ops:
  7.2 104.3 %copy-start = (bf16[1,512,2048]{2,1,0:T(8,128)(2,1)S(1)}, bf16[1,512,2048]{2,1,0:T(8,128)(2,1)}, u32[]{:S(2)}) copy-start(bf16[1,512,2048]{2,1,0:T(8,128)(2,1)} %param.40) | copy-start | bytes 6291460
  7.2 90.1 %all-reduce.2.cloned.1.call-start = ((), (), s32[]{:S(2)}) async-start(), calls=%async_computation.3 | async-start | bytes 262144 | tf_op jit(solution)/shard_map/psum | solution.py:85
  31.7 3.5 %copy-start.1 = (f32[32,2,128,128]{3,2,1,0:T(8,128)S(1)}, f32[32,2,128,128]{3,2,1,0:T(8,128)}, u32[]{:S(2)}) copy-start(f32[32,2,128,128]{3,2,1,0:T(8,128)} %param.23) | copy-start | bytes 12582916
  36.7 2.1 %copy-start.2 = (f32[32,2,128,128]{3,2,1,0:T(8,128)}, f32[32,2,128,128]{3,2,1,0:T(8,128)S(1)}, u32[]{:S(2)}) copy-start(f32[32,2,128,128]{3,2,1,0:T(8,128)S(1)} %multiply_add_fusion) | copy-start | bytes 12582916
  36.8 2.9 %copy-start.4 = (bf16[2048,256]{1,0:T(8,128)(2,1)S(1)}, bf16[2048,256]{1,0:T(8,128)(2,1)}, u32[]{:S(2)}) copy-start(bf16[2048,256]{1,0:T(8,128)(2,1)} %param.28) | copy-start | bytes 3145732
  36.8 3.3 %copy-start.10 = (bf16[128]{0:T(256)(128)(2,1)S(1)}, bf16[128]{0:T(256)(128)(2,1)}, u32[]{:S(2)}) copy-start(bf16[128]{0:T(256)(128)(2,1)} %param.33) | copy-start | bytes 772
  36.8 3.4 %copy-start.3 = (bf16[256,2048]{1,0:T(8,128)(2,1)S(1)}, bf16[256,2048]{1,0:T(8,128)(2,1)}, u32[]{:S(2)}) copy-start(bf16[256,2048]{1,0:T(8,128)(2,1)} %param.34) | copy-start | bytes 3145732
  36.8 4.4 %copy-start.7 = (bf16[2048]{0:T(1024)(128)(2,1)S(1)}, bf16[2048]{0:T(1024)(128)(2,1)}, u32[]{:S(2)}) copy-start(bf16[2048]{0:T(1024)(128)(2,1)} %param.35) | copy-start | bytes 12292
  36.8 4.4 %copy-start.8 = (s32[32,6]{0,1:T(8,128)S(1)}, s32[32,6]{0,1:T(8,128)}, u32[]{:S(2)}) copy-start(s32[32,6]{0,1:T(8,128)} %param.36) | copy-start | bytes 2308
  36.8 5.0 %copy-start.9 = (f32[32,6]{0,1:T(8,128)S(1)}, f32[32,6]{0,1:T(8,128)}, u32[]{:S(2)}) copy-start(f32[32,6]{0,1:T(8,128)} %param.37) | copy-start | bytes 2308
  100.3 17.9 %copy-start.5 = (bf16[2048,64]{0,1:T(8,128)(2,1)S(1)}, bf16[2048,64]{0,1:T(8,128)(2,1)}, u32[]{:S(2)}) copy-start(bf16[2048,64]{0,1:T(8,128)(2,1)} %param.41) | copy-start | bytes 786436
  100.3 9.1 %all-to-all-start = ((bf16[4,1,16,2048]{3,2,1,0:T(8,128)(2,1)}), bf16[4,1,16,2048]{3,2,1,0:T(8,128)(2,1)S(1)}, u32[]{:S(2)}, u32[]{:S(2)}) async-start(bf16[4,1,16,2048]{3,2,1,0:T(8,128)(2,1)} %bitcast.9), calls=%async_computation | async-start | bytes 524288 | tf_op jit(solution)/shard_map/all_to_all | solution.py:115
  114.7 8.8 %all-to-all-start.1 = ((bf16[4,1,16,2048]{3,2,1,0:T(8,128)(2,1)}), bf16[4,1,16,2048]{3,2,1,0:T(8,128)(2,1)S(1)}, u32[]{:S(2)}, u32[]{:S(2)}) async-start(bf16[4,1,16,2048]{3,2,1,0:T(8,128)(2,1)} %fusion), calls=%async_computation.1 | async-start | bytes 524288 | tf_op jit(solution)/shard_map/all_to_all | solution.py:120
  118.1 11.8 %copy-start.6 = (bf16[64,2048]{1,0:T(8,128)(2,1)S(1)}, bf16[64,2048]{1,0:T(8,128)(2,1)}, u32[]{:S(2)}) copy-start(bf16[64,2048]{1,0:T(8,128)(2,1)} %param.43) | copy-start | bytes 786436
  118.1 42.6 %reduce-scatter.2.cloned.1.call-start = ((), (), s32[]{:S(2)}) async-start(), calls=%async_computation.4 | async-start | bytes 147456 | tf_op jit(solution)/shard_map/reduce_scatter | solution.py:131
Sparse Core Ops, SparseCore 0:
  41.3 55.9 all-reduce.1
  132.1 28.5 reduce-scatter.1
where the time goes:
time: 170 us; the launch traced here: 169 us
  waiting for transfers between devices  94.3 us (55%)
  matrix products  21.4 us (13%)
  blocking collectives  16.1 us (9%)
  between operations  14.4 us (8%)
  other arithmetic  9.68 us (6%)
  starting transfers between devices  7.25 us (4%)
  local copies, waits for them, and re-layouts  5.7 us (3%)
    psum x1, waiting for transfers between devices, body(): lax.psum(partial_value.astype(jnp.bfloat16), 'tp').astype(jnp.float32)  55.1 us
    reduce_scatter x1, waiting for transfers between devices, body(): lax.psum_scatter(branch_sum.astype(jnp.bfloat16), 'tp', scatter_dimension...  28.7 us
    all_gather x1, blocking collectives, body(): full_rows = lax.all_gather(tokens, 'tp', axis=1, tiled=True)  16.1 us
    all_to_all x1, waiting for transfers between devices, body(): lax.all_to_all(outgoing, 'ep', split_axis=0, concat_axis=0, tiled=True)  5.37 us
    all_to_all x1, waiting for transfers between devices, body(): lax.all_to_all(results, 'ep', split_axis=0, concat_axis=0, tiled=True)  5.08 us
    dot_general x4, matrix products, project(): result = jnp.dot(normed_mix, weight, preferred_element_type=jnp.float32)  4.99 us
    all_to_all x1, starting transfers between devices, body(): lax.all_to_all(outgoing, 'ep', split_axis=0, concat_axis=0, tiled=True)  3.77 us
    all_to_all x1, starting transfers between devices, body(): lax.all_to_all(results, 'ep', split_axis=0, concat_axis=0, tiled=True)  3.4 us
  transfers between devices with their start and end apart: 4, of which 4 were waited for; matrix products, arithmetic and copies ran while one was open for 1% of the time, Pallas kernels for 0%

commit v1 on v0

v1 whole, which is shorter than its diff:
```python
import jax
import jax.numpy as jnp
from jax import lax
from jax.experimental import pallas as pl
from jax.experimental.pallas import tpu as pltpu
from jax.sharding import PartitionSpec as P

epsilon = 1e-06


def rms_norm(values, gain_vector):
    squares = jnp.mean(values * values, axis=-1, keepdims=True)
    return values * lax.rsqrt(squares + epsilon) * gain_vector.astype(jnp.float32)


def unit_rows(values):
    return values * lax.rsqrt(jnp.sum(values * values, axis=-1, keepdims=True) + epsilon)


def other_core(count):
    return [(index, index ^ 1) for index in range(count)]


def chip_groups(count):
    return [list(range(core, count, 2)) for core in range(2)]


def exchange_chips(blocks):
    count = lax.axis_size("tp")
    return lax.all_to_all(
        blocks, "tp", 0, 0, tiled=True, axis_index_groups=chip_groups(count)
    )


def swap_cores(block):
    return lax.ppermute(block, "tp", other_core(lax.axis_size("tp")))


def pair_sum(partial, core):
    count = lax.axis_size("tp")
    rows, columns = partial.shape
    blocks = partial.reshape(rows, count // 2, 2, columns // count).transpose(2, 1, 0, 3)
    kept = jnp.where(core == 0, blocks[0], blocks[1])
    sent = jnp.where(core == 0, blocks[1], blocks[0]).astype(jnp.bfloat16)
    return (kept + swap_cores(sent).astype(jnp.float32)).astype(jnp.bfloat16)


def scatter_sum(partial, core):
    received = exchange_chips(pair_sum(partial, core))
    return jnp.sum(received.astype(jnp.float32), axis=0)


def sum_chips(halves):
    chips = halves.shape[0]
    copies = jnp.broadcast_to(halves[None], (chips,) + halves.shape)
    received = exchange_chips(copies.reshape((chips * chips,) + halves.shape[1:]))
    received = received.reshape((chips,) + halves.shape).astype(jnp.float32)
    return jnp.sum(received, axis=0).astype(jnp.bfloat16)


def expert_block(rows, expert_gate, expert_up, expert_down):
    gate_part = jnp.einsum("sjnd,jdf->sjnf", rows, expert_gate, preferred_element_type=jnp.float32)
    up_part = jnp.einsum("sjnd,jdf->sjnf", rows, expert_up, preferred_element_type=jnp.float32)
    hidden = (jax.nn.silu(gate_part) * up_part).astype(jnp.bfloat16)
    outputs = jnp.einsum("sjnf,jfd->sjnd", hidden, expert_down, preferred_element_type=jnp.float32)
    return outputs.astype(jnp.bfloat16)


def ordered(own_ref, theirs_ref, chip, core):
    own = own_ref[chip].astype(jnp.float32)
    theirs = theirs_ref[chip].astype(jnp.float32)
    return [jnp.where(core == 0, own, theirs), jnp.where(core == 0, theirs, own)]


def split_store(full, width, core, kept_ref, sent_ref):
    for chip in range(kept_ref.shape[0]):
        first = full[:, 2 * chip * width : (2 * chip + 1) * width]
        second = full[:, (2 * chip + 1) * width : (2 * chip + 2) * width]
        kept_ref[chip] = jnp.where(core == 0, first, second)
        sent_ref[chip] = jnp.where(core == 0, second, first).astype(jnp.bfloat16)


def mixer_kernel(
    place_ref, scale_ref, bias_ref, own_ref, theirs_ref, gain_ref, beta_ref, decay_ref, head_gain_ref,
    query_hbm, key_hbm, value_hbm, gate_hbm, output_hbm, state_hbm,
    new_hbm, kept_ref, sent_ref, rows_ref,
    weights, output_weight, state, sems,
):
    core = place_ref[0] % 2
    rows_count, heads_here, key_size, value_size = state.shape
    chips, _, width = own_ref.shape
    group = 8
    chunks = rows_count // group
    weight_copies = [
        pltpu.make_async_copy(source, weights.at[index], sems.at[index])
        for index, source in enumerate((key_hbm, query_hbm, value_hbm, gate_hbm))
    ]
    output_copy = pltpu.make_async_copy(output_hbm, output_weight, sems.at[4])
    reads = [
        pltpu.make_async_copy(
            state_hbm.at[pl.ds(group * c, group)], state.at[pl.ds(group * c, group)], sems.at[5 + c]
        )
        for c in range(chunks)
    ]
    writes = [
        pltpu.make_async_copy(
            state.at[pl.ds(group * c, group)],
            new_hbm.at[pl.ds(group * c, group)],
            sems.at[5 + chunks + c],
        )
        for c in range(chunks)
    ]
    for copy in weight_copies[:3] + reads + [weight_copies[3], output_copy]:
        copy.start()
    pieces = []
    for chip in range(chips):
        pieces += ordered(own_ref, theirs_ref, chip, core)
    resid = jnp.concatenate(pieces, axis=1)
    rows_ref[...] = resid.astype(jnp.bfloat16)
    normed_wide = rms_norm(resid, gain_ref[...])
    normed = normed_wide.astype(jnp.bfloat16)
    normed_wide = normed.astype(jnp.float32)

    def project(index):
        weight_copies[index].wait()
        result = jnp.dot(normed, weights[index], preferred_element_type=jnp.float32)
        return result.astype(jnp.bfloat16).astype(jnp.float32)

    betas, decays = [], []
    for head in range(heads_here):
        beta_in = jnp.sum(
            normed_wide * beta_ref[head : head + 1, :].astype(jnp.float32), axis=1, keepdims=True
        )
        decay_in = jnp.sum(
            normed_wide * decay_ref[head : head + 1, :].astype(jnp.float32), axis=1, keepdims=True
        ) + bias_ref[head]
        soft = jnp.maximum(decay_in, 0.0) + jnp.log1p(jnp.exp(-jnp.abs(decay_in)))
        betas.append(1.0 / (1.0 + jnp.exp(-beta_in)))
        decays.append(jnp.broadcast_to(jnp.exp(-scale_ref[head] * soft), (rows_count, value_size)))
    keys_all = project(0)
    queries_all = project(1)
    values_all = project(2)
    heads = range(heads_here)
    cut = lambda array, head, size: array[:, head * size : (head + 1) * size]
    keys = [unit_rows(cut(keys_all, head, key_size)) for head in heads]
    queries = [unit_rows(cut(queries_all, head, key_size)) * key_size ** (-0.5) for head in heads]
    values = [cut(values_all, head, value_size) for head in heads]
    mixes = [jnp.sum(keys[head] * queries[head], axis=1, keepdims=True) for head in heads]
    key_columns = [keys[head].T for head in heads]
    query_columns = [queries[head].T for head in heads]
    state_reads = [[] for _ in heads]
    for c in range(chunks):
        reads[c].wait()
        low, high = group * c, group * (c + 1)
        for head in heads:
            key_parts, query_parts = [], []
            for s in range(low, high):
                old = state[s, head]
                key_parts.append(
                    jnp.sum(old * key_columns[head][:, s : s + 1], axis=0, keepdims=True)
                )
                query_parts.append(
                    jnp.sum(old * query_columns[head][:, s : s + 1], axis=0, keepdims=True)
                )
            decay = decays[head][low:high]
            change = betas[head][low:high] * (
                values[head][low:high] - decay * jnp.concatenate(key_parts, axis=0)
            )
            state_reads[head].append(
                decay * jnp.concatenate(query_parts, axis=0) + mixes[head][low:high] * change
            )
            for s in range(low, high):
                at = s - low
                state[s, head] = (
                    decay[at : at + 1] * state[s, head]
                    + key_columns[head][:, s : s + 1] * change[at : at + 1]
                )
        writes[c].start()
    gates_all = project(3)
    gated = []
    for head in heads:
        gate = cut(gates_all, head, value_size)
        normal = rms_norm(jnp.concatenate(state_reads[head], axis=0), head_gain_ref[...])
        gated.append((normal * (gate / (1.0 + jnp.exp(-gate)))).astype(jnp.bfloat16))
    output_copy.wait()
    partial = jnp.dot(
        jnp.concatenate(gated, axis=1), output_weight[...], preferred_element_type=jnp.float32
    )
    split_store(partial, width, core, kept_ref, sent_ref)
    for copy in writes:
        copy.wait()


def mixer(place, own, theirs, delta_state, mix_gain, w_query, w_key, w_value, w_outgate, w_beta,
          w_decay, decay_scale, decay_bias, head_gain, w_output):
    chips, rows_count, width = own.shape
    columns = w_query.shape[0]
    vmem = pl.BlockSpec(memory_space=pltpu.VMEM)
    smem = pl.BlockSpec(memory_space=pltpu.SMEM)
    hbm = pl.BlockSpec(memory_space=pltpu.HBM)
    return pl.pallas_call(
        mixer_kernel,
        name="mixer",
        in_specs=[smem] * 3 + [vmem] * 6 + [hbm] * 6,
        out_specs=[hbm, vmem, vmem, vmem],
        out_shape=[
            pltpu.HBM(delta_state.shape, jnp.float32),
            jax.ShapeDtypeStruct((chips, rows_count, width), jnp.float32),
            jax.ShapeDtypeStruct((chips, rows_count, width), jnp.bfloat16),
            jax.ShapeDtypeStruct((rows_count, columns), jnp.bfloat16),
        ],
        scratch_shapes=[
            pltpu.VMEM((4,) + w_query.shape, jnp.bfloat16),
            pltpu.VMEM(w_output.shape, jnp.bfloat16),
            pltpu.VMEM(delta_state.shape, jnp.float32),
            pltpu.SemaphoreType.DMA((5 + 2 * (rows_count // 8),)),
        ],
        compiler_params=pltpu.CompilerParams(vmem_limit_bytes=40 * 2**20),
    )(
        place, decay_scale, decay_bias, own, theirs, mix_gain[None], w_beta.T, w_decay.T,
        head_gain[None],
        *[pltpu.with_memory_space_constraint(array, pltpu.HBM)
          for array in (w_query, w_key, w_value, w_outgate, w_output, delta_state)],
    )


def dispatch_kernel(
    place_ref, own_ref, theirs_ref, rows_ref, gain_ref, choose_ref, outgoing_ref, normed_ref, resid_ref
):
    core = place_ref[0] % 2
    chips, _, width = own_ref.shape
    pieces = []
    for chip in range(chips):
        pieces += ordered(own_ref, theirs_ref, chip, core)
    resid = jnp.concatenate(pieces, axis=1) + rows_ref[...].astype(jnp.float32)
    normed = rms_norm(resid, gain_ref[...]).astype(jnp.bfloat16)
    normed_ref[...] = normed
    outgoing = jnp.dot(choose_ref[...], normed, preferred_element_type=jnp.float32)
    outgoing_ref[...] = outgoing.astype(jnp.bfloat16)
    here = jnp.zeros(resid_ref.shape, jnp.float32)
    for block in range(2 * chips):
        here = jnp.where(place_ref[0] == block, resid[:, block * width : (block + 1) * width], here)
    resid_ref[...] = here


def dispatch(place, own, theirs, rows, gain, choose):
    vmem = pl.BlockSpec(memory_space=pltpu.VMEM)
    smem = pl.BlockSpec(memory_space=pltpu.SMEM)
    return pl.pallas_call(
        dispatch_kernel,
        name="dispatch",
        in_specs=[smem] + [vmem] * 5,
        out_specs=[vmem] * 3,
        out_shape=[
            jax.ShapeDtypeStruct((choose.shape[0], rows.shape[1]), jnp.bfloat16),
            jax.ShapeDtypeStruct(rows.shape, jnp.bfloat16),
            jax.ShapeDtypeStruct(own.shape[1:], jnp.float32),
        ],
    )(place, own, theirs, rows, gain[None], choose)


def body(
    tokens,
    delta_state,
    mix_gain,
    w_query,
    w_key,
    w_value,
    w_outgate,
    w_beta,
    w_decay,
    decay_scale,
    decay_bias,
    head_gain,
    w_output,
    ffn_gain,
    route_ids,
    route_weights,
    expert_gate,
    expert_up,
    expert_down,
    shared_gate,
    shared_up,
    shared_down,
):
    rows_count = tokens.shape[0]
    heads_here = delta_state.shape[1]
    tp_index = lax.axis_index("tp")
    core = tp_index % 2
    place = tp_index[None]
    chips = lax.axis_size("tp") // 2
    own_rows = exchange_chips(jnp.broadcast_to(tokens[None], (chips,) + tokens.shape))
    new_state, kept, sent, full_rows = mixer(
        place, own_rows, swap_cores(own_rows), delta_state, mix_gain, w_query, w_key, w_value,
        w_outgate, w_beta, w_decay, decay_scale, decay_bias, head_gain, w_output,
    )
    halves = (kept + swap_cores(sent).astype(jnp.float32)).astype(jnp.bfloat16)
    mixed = sum_chips(halves)
    model_width = full_rows.shape[1]
    ep_count = lax.axis_size("ep")
    tp_count = lax.axis_size("tp")
    experts_here = expert_gate.shape[0]
    top_count = route_ids.shape[1]
    expert_total = experts_here * ep_count * tp_count
    capacity = max(2, 8 * rows_count * top_count // (3 * expert_total))
    pair_count = rows_count * top_count
    flat_ids = route_ids.reshape(pair_count)
    owner_ep = flat_ids // (tp_count * experts_here)
    owner_tp = flat_ids // experts_here % tp_count
    local_slot = flat_ids % experts_here
    mine_mask = owner_tp == tp_index
    pair_weights = jnp.where(mine_mask, route_weights.reshape(pair_count), 0.0)
    pair_index = jnp.arange(pair_count, dtype=jnp.int32)
    earlier = (flat_ids[:, None] == flat_ids[None, :]) & (pair_index[None, :] < pair_index[:, None])
    slot_rank = jnp.sum(earlier.astype(jnp.int32), axis=1)
    slot_count = ep_count * experts_here * capacity
    target = jnp.where(mine_mask, (owner_ep * experts_here + local_slot) * capacity + slot_rank, -1)
    choose = (target[:, None] == jnp.arange(slot_count, dtype=jnp.int32)[None, :]).astype(
        jnp.bfloat16
    )
    by_row = jnp.sum(choose.reshape(rows_count, top_count, slot_count), axis=1)
    outgoing, normed_ffn, resid_own = dispatch(
        place, mixed, swap_cores(mixed), full_rows, ffn_gain, by_row.T
    )
    outgoing = outgoing.reshape(ep_count, experts_here, capacity, model_width)
    results = expert_block(
        lax.all_to_all(outgoing, "ep", split_axis=0, concat_axis=0, tiled=True),
        expert_gate,
        expert_up,
        expert_down,
    )
    returned = lax.all_to_all(results, "ep", split_axis=0, concat_axis=0, tiled=True)
    weights_of = jnp.sum(
        jnp.where(choose > 0, pair_weights[:, None], 0.0).reshape(rows_count, top_count, slot_count),
        axis=1,
    )
    weights_high = weights_of.astype(jnp.bfloat16)
    weights_low = (weights_of - weights_high.astype(jnp.float32)).astype(jnp.bfloat16)
    returned = returned.reshape(slot_count, model_width)
    routed = jnp.dot(
        jnp.concatenate([weights_high, weights_low], axis=1),
        jnp.concatenate([returned, returned], axis=0),
        preferred_element_type=jnp.float32,
    )
    shared_gate_part = jnp.dot(normed_ffn, shared_gate, preferred_element_type=jnp.float32)
    shared_up_part = jnp.dot(normed_ffn, shared_up, preferred_element_type=jnp.float32)
    hidden_shared = (jax.nn.silu(shared_gate_part) * shared_up_part).astype(jnp.bfloat16)
    branch_sum = routed + jnp.dot(hidden_shared, shared_down, preferred_element_type=jnp.float32)
    combined = scatter_sum(branch_sum, core)
    layer_out = (resid_own + combined).astype(jnp.bfloat16)
    return (layer_out, new_state)


def solution(mesh):
    return jax.shard_map(
        body,
        mesh=mesh,
        in_specs=(
            P("ep", "tp"),
            P("ep", "tp", None, None),
            P(),
            P(None, "tp"),
            P(None, "tp"),
            P(None, "tp"),
            P(None, "tp"),
            P(None, "tp"),
            P(None, "tp"),
            P("tp"),
            P("tp"),
            P(),
            P("tp", None),
            P(),
            P("ep", None),
            P("ep", None),
            P(("ep", "tp"), None, None),
            P(("ep", "tp"), None, None),
            P(("ep", "tp"), None, None),
            P(None, "tp"),
            P(None, "tp"),
            P("tp", None),
        ),
        out_specs=(P("ep", "tp"), P("ep", "tp", None, None)),
        check_vma=False,
    )
```

time: 170 us -> 81.4 us (0.48)
  waiting for transfers between devices: 94.3 us -> 26.3 us
  matrix products: 21.4 us -> 7.07 us
  between operations: 14.4 us -> 0.9 us
  starting transfers between devices: 7.25 us -> 17.3 us
  Pallas kernels: 0 us -> 9.15 us
  other arithmetic: 9.68 us -> 1.16 us
  blocking collectives: 16.1 us -> 8.27 us
  local copies, waits for them, and re-layouts: 5.7 us -> 10.4 us
    psum x1 -> x0, waiting for transfers between devices: 55.1 us -> none  [body(): lax.psum(partial_value.astype(jnp.bfloat16), 'tp').astype(jnp.float32)]
    reduce_scatter x1 -> x0, waiting for transfers between devices: 28.7 us -> none  [body(): lax.psum_scatter(branch_sum.astype(jnp.bfloat16), 'tp', scatter_dimension...]
    all_gather x1 -> x0, blocking collectives: 16.1 us -> none  [body(): full_rows = lax.all_gather(tokens, 'tp', axis=1, tiled=True)]
    dot_general x11 -> x1, matrix products: 14 us -> 0.25 us  [body(): jnp.dot(jnp.concatenate([weights_high, weights_low], axis=1), jnp.concate...]
    all_to_all x0 -> x2, waiting for transfers between devices: none -> 13.3 us  [exchange_chips(): lax.all_to_all(blocks, 'tp', 0, 0, tiled=True, axis_index_groups=chip_gro...]
    all_to_all x0 -> x2, starting transfers between devices: none -> 9.75 us  [exchange_chips(): lax.all_to_all(blocks, 'tp', 0, 0, tiled=True, axis_index_groups=chip_gro...]
    pallas_call x0 -> x2, Pallas kernels: none -> 9.15 us  [the longest x1 7.1 us: mixer(): pl.pallas_call(mixer_kernel, name='mixer', in_specs=[smem] * 3 + [vmem] *...]
    all_to_all x0 -> x1, blocking collectives: none -> 8.27 us  [exchange_chips(): lax.all_to_all(blocks, 'tp', 0, 0, tiled=True, axis_index_groups=chip_gro...]
  transfers between devices with their start and end apart: 4 -> 8, of which waited for: 4 -> 7; matrix products, arithmetic and copies ran while one was open for 1% -> 6% of each run, Pallas kernels for 0% -> 0%
where the time goes in v1:
time: 81.4 us; the launch traced here: 80.6 us
  waiting for transfers between devices  26.3 us (32%)
  starting transfers between devices  17.3 us (21%)
  local copies, waits for them, and re-layouts  10.4 us (13%)
  Pallas kernels  9.15 us (11%)
  blocking collectives  8.27 us (10%)
  matrix products  7.07 us (9%)
  other arithmetic  1.16 us (1%)
  between operations  0.9 us (1%)
    all_to_all x2, waiting for transfers between devices, exchange_chips(): lax.all_to_all(blocks, 'tp', 0, 0, tiled=True, axis_index_groups=chip_gro...  13.3 us
    all_to_all x2, starting transfers between devices, exchange_chips(): lax.all_to_all(blocks, 'tp', 0, 0, tiled=True, axis_index_groups=chip_gro...  9.75 us
    all_to_all x1, blocking collectives, exchange_chips(): lax.all_to_all(blocks, 'tp', 0, 0, tiled=True, axis_index_groups=chip_gro...  8.27 us
    pallas_call x1, Pallas kernels, mixer(): pl.pallas_call(mixer_kernel, name='mixer', in_specs=[smem] * 3 + [vmem] *...  7.1 us
    unnamed x34, local copies, waits for them, and re-layouts  5.53 us
    all_to_all x1, waiting for transfers between devices, body(): lax.all_to_all(outgoing, 'ep', split_axis=0, concat_axis=0, tiled=True)  4.94 us
    all_to_all x1, waiting for transfers between devices, body(): lax.all_to_all(results, 'ep', split_axis=0, concat_axis=0, tiled=True)  4.89 us
    all_to_all x1, starting transfers between devices, body(): lax.all_to_all(outgoing, 'ep', split_axis=0, concat_axis=0, tiled=True)  3.72 us
  transfers between devices with their start and end apart: 8, of which 7 were waited for; matrix products, arithmetic and copies ran while one was open for 6% of the time, Pallas kernels for 0%

profile of v1, /device:TPU:0, one launch (start us, length us, event | category | flops | bytes accessed | tf_op | source)
XLA Modules:
  0.0 80.6 jit_solution(17116001899646013278)
XLA Ops:
  0.6 0.0 copy-start
  0.6 1.5 %broadcast_in_dim.48 = bf16[4,32,256]{2,1,0:T(8,128)(2,1)} broadcast(bf16[32,256]{1,0:T(8,128)(2,1)} %param.22), dimensions={1,2} | broadcast | bytes 81920 | tf_op jit(solution)/shard_map/broadcast_in_dim | solution.py:292
  2.1 6.3 %all-to-all-start = ((bf16[4,32,256]{2,1,0:T(8,128)(2,1)}), bf16[4,32,256]{2,1,0:T(8,128)(2,1)S(1)}, u32[]{:S(2)}, u32[]{:S(2)}) async-start(bf16[4,32,256]{2,1,0:T(8,128)(2,1)} %broadcast_in_dim.48), calls=%async_computation | async-start | bytes 131072 | tf_op jit(solution)/shard_map/all_to_all | solution.py:30
  8.5 0.7 broadcast_in_dim.49.gain_ref
  9.2 0.8 copy.46
  10.0 0.1 eq.54
  10.1 4.2 %all-to-all-done.own_ref = bf16[4,32,256]{2,1,0:T(8,128)(2,1)S(1)} async-done(((bf16[4,32,256]{2,1,0:T(8,128)(2,1)}), bf16[4,32,256]{2,1,0:T(8,128)(2,1)S(1)}, u32[]{:S(2)}, u32[]{:S(2)}) %all-to-all-start) | async-done | bytes 65568 | tf_op jit(solution)/shard_map/all_to_all | solution.py:30
  14.2 0.0 collective-permute-start
  14.2 0.2 convert_reduce_fusion
  14.4 0.1 reduce_sum.55
  14.5 1.0 %collective-permute-done.theirs_ref = bf16[4,32,256]{2,1,0:T(8,128)(2,1)S(1)} collective-permute-done((bf16[4,32,256]{2,1,0:T(8,128)(2,1)S(1)}, bf16[4,32,256]{2,1,0:T(8,128)(2,1)S(1)}, u32[]{:S(2)}, u32[]{:S(2)}) %collective-permute-start) | collective-permute-done | bytes 65568 | tf_op jit(solution)/shard_map/ppermute | solution.py:36
  15.5 0.0 copy-start.2
  15.5 0.7 copy-done.2
  16.2 0.7 copy-done.3
  16.9 0.7 copy-done.4
  17.5 0.7 copy-done.5
  18.2 0.7 copy-done.6
  18.9 7.1 %mixer.1 = (f32[32,2,128,128]{3,2,1,0:T(8,128)}, f32[4,32,256]{2,1,0:T(8,128)S(1)}, bf16[4,32,256]{2,1,0:T(8,128)(2,1)S(1)}, bf16[32,2048]{1,0:T(8,128)(2,1)S(1)}) custom-call(s32[1]{0:T(128)} %bitcast.place_ref, f32[2]{0:T(128)S(1)} %copy-done.4, f32[2]{0:T(128)S(1)} %copy-done.5, bf16[4,32,256]{2,1,0:T(8,128)(2,1)S(1)} %all-to-all-done.own_ref, ...), custom_call_target="tpu_custom_call" | custom-call | tf_op jit(solution)/shard_map/mixer/pallas_call | solution.py:201
  26.0 0.0 copy-start.1
  26.0 0.6 copy-done.1
  26.6 0.2 collective-permute-start.1
  26.8 0.0 copy-done.14
  26.8 0.1 copy.53
  26.9 1.0 %collective-permute-done.1 = bf16[4,32,256]{2,1,0:T(8,128)(2,1)S(1)} collective-permute-done((bf16[4,32,256]{2,1,0:T(8,128)(2,1)S(1)}, bf16[4,32,256]{2,1,0:T(8,128)(2,1)S(1)}, u32[]{:S(2)}, u32[]{:S(2)}) %collective-permute-start.1) | collective-permute-done | bytes 65568 | tf_op jit(solution)/shard_map/ppermute | solution.py:36
  27.9 0.7 broadcast_in_dim.51
  28.6 3.4 %all-to-all-start.1 = ((bf16[16,32,256]{2,1,0:T(8,128)(2,1)}), bf16[16,32,256]{2,1,0:T(8,128)(2,1)S(1)}, u32[]{:S(2)}, u32[]{:S(2)}) async-start(bf16[16,32,256]{2,1,0:T(8,128)(2,1)} %bitcast.4), calls=%async_computation.1 | async-start | bytes 524288 | tf_op jit(solution)/shard_map/all_to_all | solution.py:30
  32.1 0.1 copy.51
  32.1 0.1 copy.54
  32.2 0.1 select_reduce_fusion
  32.4 9.1 %all-to-all-done.1 = bf16[16,32,256]{2,1,0:T(8,128)(2,1)S(1)} async-done(((bf16[16,32,256]{2,1,0:T(8,128)(2,1)}), bf16[16,32,256]{2,1,0:T(8,128)(2,1)S(1)}, u32[]{:S(2)}, u32[]{:S(2)}) %all-to-all-start.1) | async-done | bytes 262176 | tf_op jit(solution)/shard_map/all_to_all | solution.py:30
  41.5 0.0 copy-start.11
  41.5 0.1 collective-permute-start.2
  41.6 0.1 fusion.37
  41.7 0.7 copy.52
  42.4 0.0 copy-done.15
  42.4 0.6 broadcast_in_dim.52.gain_ref
  43.0 0.0 collective-permute-done.2.theirs_ref
  43.0 0.0 copy-done.11
  43.0 0.6 copy-done.12
  43.6 2.0 %dispatch.1 = (bf16[64,2048]{1,0:T(8,128)(2,1)}, bf16[32,2048]{1,0:T(8,128)(2,1)}, f32[32,256]{1,0:T(8,128)}) custom-call(s32[1]{0:T(128)} %bitcast.place_ref, bf16[4,32,256]{2,1,0:T(8,128)(2,1)} %copy-done.11, bf16[4,32,256]{2,1,0:T(8,128)(2,1)} %copy-done.12, bf16[32,2048]{1,0:T(8,128)(2,1)} %copy-done.1, bf16[1,2048]{1,0:T(2,128)(2,1)} %broadcast_in_dim.52.gain_ref, ...), custom_call_target="tpu_custom_call" | custom-call | tf_op jit(solution)/shard_map/dispatch/pallas_call | solution.py:249
  45.7 3.7 %all-to-all-start.2 = ((bf16[4,1,16,2048]{3,2,1,0:T(8,128)(2,1)}), bf16[4,1,16,2048]{3,2,1,0:T(8,128)(2,1)S(1)}, u32[]{:S(2)}, u32[]{:S(2)}) async-start(bf16[4,1,16,2048]{3,2,1,0:T(8,128)(2,1)} %bitcast.94), calls=%async_computation.2 | async-start | bytes 524288 | tf_op jit(solution)/shard_map/all_to_all | solution.py:327
  49.4 0.0 copy-done.10
  49.4 1.1 %fusion.56 = f32[32,64]{1,0:T(8,128)S(1)} fusion(bf16[32,2048]{1,0:T(8,128)(2,1)} %get-tuple-element.14, bf16[2048,64]{0,1:T(8,128)(2,1)S(1)} %copy-done.10), kind=kOutput, calls=%fused_computation.63 | convolution fusion | flops 8388608 | bytes 401408 | tf_op jit(solution)/shard_map/dot_general | solution.py:345
  50.5 4.9 %all-to-all-done.2 = bf16[4,1,16,2048]{3,2,1,0:T(8,128)(2,1)S(1)} async-done(((bf16[4,1,16,2048]{3,2,1,0:T(8,128)(2,1)}), bf16[4,1,16,2048]{3,2,1,0:T(8,128)(2,1)S(1)}, u32[]{:S(2)}, u32[]{:S(2)}) %all-to-all-start.2) | async-done | bytes 262176 | tf_op jit(solution)/shard_map/all_to_all | solution.py:327
  55.4 2.1 %fusion.6 = f32[4,1,16,512]{3,2,0,1:T(8,128)S(1)} fusion(bf16[1,2048,512]{2,1,0:T(8,128)(2,1)} %param.38, bf16[4,1,16,2048]{3,2,1,0:T(8,128)(2,1)S(1)} %all-to-all-done.2), kind=kOutput, calls=%fused_computation.8 | convolution fusion | flops 134217728 | bytes 2490368 | tf_op jit(solution)/shard_map/sjnd,jdf->sjnf/dot_general | solution.py:62
  57.5 0.0 copy-done
  57.5 0.0 copy-start.7
  57.5 0.0 copy-start.8
  57.5 0.0 copy-start.9
  57.5 3.3 %fusion = bf16[4,1,16,2048]{3,2,1,0:T(8,128)(2,1)} fusion(bf16[1,512,2048]{2,1,0:T(8,128)(2,1)S(1)} %copy-done, bf16[1,2048,512]{2,1,0:T(8,128)(2,1)} %param.39, bf16[4,1,16,2048]{3,2,1,0:T(8,128)(2,1)S(1)} %all-to-all-done.2, f32[4,1,16,512]{3,2,0,1:T(8,128)S(1)} %fusion.6), kind=kOutput, calls=%fused_computation.1 | convolution fusion | flops 268763136 | bytes 4849664 | tf_op jit(solution)/shard_map/sjnf,jfd->sjnd/dot_general | solution.py:65
  60.8 3.5 %all-to-all-start.3 = ((bf16[4,1,16,2048]{3,2,1,0:T(8,128)(2,1)}), bf16[4,1,16,2048]{3,2,1,0:T(8,128)(2,1)S(1)}, u32[]{:S(2)}, u32[]{:S(2)}) async-start(bf16[4,1,16,2048]{3,2,1,0:T(8,128)(2,1)} %fusion), calls=%async_computation.3 | async-start | bytes 524288 | tf_op jit(solution)/shard_map/all_to_all | solution.py:332
  64.4 0.0 copy-done.7
  64.4 0.0 copy-done.8
  64.4 0.0 copy-done.9
  64.4 0.4 fusion.46
  64.8 4.9 %all-to-all-done.3 = bf16[4,1,16,2048]{3,2,1,0:T(8,128)(2,1)S(1)} async-done(((bf16[4,1,16,2048]{3,2,1,0:T(8,128)(2,1)}), bf16[4,1,16,2048]{3,2,1,0:T(8,128)(2,1)S(1)}, u32[]{:S(2)}, u32[]{:S(2)}) %all-to-all-start.3) | async-done | bytes 262176 | tf_op jit(solution)/shard_map/all_to_all | solution.py:332
  69.7 0.3 convolution_add_fusion
  70.0 0.2 reshape.140
  70.2 0.1 copy.59
  70.3 0.1 collective-permute-start.3
  70.4 1.2 %collective-permute-done.3 = bf16[4,32,256]{2,1,0:T(8,128)(2,1)S(1)} collective-permute-done((bf16[4,32,256]{2,1,0:T(8,128)(2,1)S(1)}, bf16[4,32,256]{2,1,0:T(8,128)(2,1)S(1)}, u32[]{:S(2)}, u32[]{:S(2)}) %collective-permute-start.3) | collective-permute-done | bytes 65568 | tf_op jit(solution)/shard_map/ppermute | solution.py:36
  71.6 8.3 %all_to_all.25 = bf16[4,32,256]{2,1,0:T(8,128)(2,1)S(1)} all-to-all(bf16[4,32,256]{2,1,0:T(8,128)(2,1)S(1)} %fusion.30), channel_id=1, replica_groups={{0,2,4,6},{1,3,5,7},{8,10,12,14},{9,11,13,15},{16,18,20,22},{17,19,21,2..., dimensions={0} | all-to-all | bytes 131072 | tf_op jit(solution)/shard_map/all_to_all | solution.py:30
  79.9 0.0 copy-done.13
  79.9 0.6 add_convert_fusion.1
  (17 shorter events, 0.2 us)
Async XLA Ops:
  0.6 56.9 %copy-start = (bf16[1,512,2048]{2,1,0:T(8,128)(2,1)S(1)}, bf16[1,512,2048]{2,1,0:T(8,128)(2,1)}, u32[]{:S(2)}) copy-start(bf16[1,512,2048]{2,1,0:T(8,128)(2,1)} %param.40) | copy-start | bytes 6291460
  2.1 12.1 %all-to-all-start = ((bf16[4,32,256]{2,1,0:T(8,128)(2,1)}), bf16[4,32,256]{2,1,0:T(8,128)(2,1)S(1)}, u32[]{:S(2)}, u32[]{:S(2)}) async-start(bf16[4,32,256]{2,1,0:T(8,128)(2,1)} %broadcast_in_dim.48), calls=%async_computation | async-start | bytes 131072 | tf_op jit(solution)/shard_map/all_to_all | solution.py:30
  14.2 1.3 %collective-permute-start = (bf16[4,32,256]{2,1,0:T(8,128)(2,1)S(1)}, bf16[4,32,256]{2,1,0:T(8,128)(2,1)S(1)}, u32[]{:S(2)}, u32[]{:S(2)}) collective-permute-start(bf16[4,32,256]{2,1,0:T(8,128)(2,1)S(1)} %all-to-all-done.own_ref), channel_id=1, source_target_pairs={{0,1},{1,0},{2,3},{3,2},{4,5},{5,4},{6,7},{7,6},{8,9},{9,8},{10,11... | collective-permute-start | bytes 196616 | tf_op jit(solution)/shard_map/ppermute | solution.py:36
  15.5 0.7 copy-start.2
  16.2 0.7 copy-start.3
  16.9 0.7 copy-start.4
  17.5 0.7 copy-start.5
  18.2 0.7 copy-start.6
  18.9 8.0 %copy-start.14 = (f32[32,6]{0,1:T(8,128)S(1)}, f32[32,6]{0,1:T(8,128)}, u32[]{:S(2)}) copy-start(f32[32,6]{0,1:T(8,128)} %param.37) | copy-start | bytes 2308
  18.9 23.6 %copy-start.15 = (bf16[2048]{0:T(1024)(128)(2,1)S(1)}, bf16[2048]{0:T(1024)(128)(2,1)}, u32[]{:S(2)}) copy-start(bf16[2048]{0:T(1024)(128)(2,1)} %param.35) | copy-start | bytes 12292
  26.0 0.7 copy-start.1
  26.6 22.8 %copy-start.10 = (bf16[2048,64]{0,1:T(8,128)(2,1)S(1)}, bf16[2048,64]{0,1:T(8,128)(2,1)}, u32[]{:S(2)}) copy-start(bf16[2048,64]{0,1:T(8,128)(2,1)} %param.41) | copy-start | bytes 786436
  26.6 1.3 %collective-permute-start.1 = (bf16[4,32,256]{2,1,0:T(8,128)(2,1)S(1)}, bf16[4,32,256]{2,1,0:T(8,128)(2,1)S(1)}, u32[]{:S(2)}, u32[]{:S(2)}) collective-permute-start(bf16[4,32,256]{2,1,0:T(8,128)(2,1)S(1)} %get-tuple-element.10), channel_id=1, source_target_pairs={{0,1},{1,0},{2,3},{3,2},{4,5},{5,4},{6,7},{7,6},{8,9},{9,8},{10,11... | collective-permute-start | bytes 196616 | tf_op jit(solution)/shard_map/ppermute | solution.py:36
  28.6 12.9 %all-to-all-start.1 = ((bf16[16,32,256]{2,1,0:T(8,128)(2,1)}), bf16[16,32,256]{2,1,0:T(8,128)(2,1)S(1)}, u32[]{:S(2)}, u32[]{:S(2)}) async-start(bf16[16,32,256]{2,1,0:T(8,128)(2,1)} %bitcast.4), calls=%async_computation.1 | async-start | bytes 524288 | tf_op jit(solution)/shard_map/all_to_all | solution.py:30
  41.5 1.5 %copy-start.11 = (bf16[4,32,256]{2,1,0:T(8,128)(2,1)}, bf16[4,32,256]{2,1,0:T(8,128)(2,1)S(1)}, u32[]{:S(2)}) copy-start(bf16[4,32,256]{2,1,0:T(8,128)(2,1)S(1)} %reduce_sum.53.own_ref) | copy-start | bytes 196612
  41.5 1.5 %collective-permute-start.2 = (bf16[4,32,256]{2,1,0:T(8,128)(2,1)S(1)}, bf16[4,32,256]{2,1,0:T(8,128)(2,1)S(1)}, u32[]{:S(2)}, u32[]{:S(2)}) collective-permute-start(bf16[4,32,256]{2,1,0:T(8,128)(2,1)S(1)} %reduce_sum.53.own_ref), channel_id=1, source_target_pairs={{0,1},{1,0},{2,3},{3,2},{4,5},{5,4},{6,7},{7,6},{8,9},{9,8},{10,11... | collective-permute-start | bytes 196616 | tf_op jit(solution)/shard_map/ppermute | solution.py:36
  43.0 0.6 copy-start.12
  45.7 9.7 %all-to-all-start.2 = ((bf16[4,1,16,2048]{3,2,1,0:T(8,128)(2,1)}), bf16[4,1,16,2048]{3,2,1,0:T(8,128)(2,1)S(1)}, u32[]{:S(2)}, u32[]{:S(2)}) async-start(bf16[4,1,16,2048]{3,2,1,0:T(8,128)(2,1)} %bitcast.94), calls=%async_computation.2 | async-start | bytes 524288 | tf_op jit(solution)/shard_map/all_to_all | solution.py:327
  57.5 6.8 %copy-start.7 = (bf16[32,2048]{1,0:T(8,128)(2,1)S(1)}, bf16[32,2048]{1,0:T(8,128)(2,1)}, u32[]{:S(2)}) copy-start(bf16[32,2048]{1,0:T(8,128)(2,1)} %get-tuple-element.14) | copy-start | bytes 393220
  57.5 6.8 %copy-start.8 = (bf16[64,2048]{1,0:T(8,128)(2,1)S(1)}, bf16[64,2048]{1,0:T(8,128)(2,1)}, u32[]{:S(2)}) copy-start(bf16[64,2048]{1,0:T(8,128)(2,1)} %param.43) | copy-start | bytes 786436
  57.5 6.8 %copy-start.9 = (bf16[2048,64]{0,1:T(8,128)(2,1)S(1)}, bf16[2048,64]{0,1:T(8,128)(2,1)}, u32[]{:S(2)}) copy-start(bf16[2048,64]{0,1:T(8,128)(2,1)} %param.42) | copy-start | bytes 786436
  60.8 19.1 %copy-start.13 = (f32[32,256]{1,0:T(8,128)S(1)}, f32[32,256]{1,0:T(8,128)}, u32[]{:S(2)}) copy-start(f32[32,256]{1,0:T(8,128)} %get-tuple-element.12) | copy-start | bytes 98308
  60.8 8.9 %all-to-all-start.3 = ((bf16[4,1,16,2048]{3,2,1,0:T(8,128)(2,1)}), bf16[4,1,16,2048]{3,2,1,0:T(8,128)(2,1)S(1)}, u32[]{:S(2)}, u32[]{:S(2)}) async-start(bf16[4,1,16,2048]{3,2,1,0:T(8,128)(2,1)} %fusion), calls=%async_computation.3 | async-start | bytes 524288 | tf_op jit(solution)/shard_map/all_to_all | solution.py:332
  70.3 1.3 %collective-permute-start.3 = (bf16[4,32,256]{2,1,0:T(8,128)(2,1)S(1)}, bf16[4,32,256]{2,1,0:T(8,128)(2,1)S(1)}, u32[]{:S(2)}, u32[]{:S(2)}) collective-permute-start(bf16[4,32,256]{2,1,0:T(8,128)(2,1)S(1)} %fusion.38), channel_id=1, source_target_pairs={{0,1},{1,0},{2,3},{3,2},{4,5},{5,4},{6,7},{7,6},{8,9},{9,8},{10,11... | collective-permute-start | bytes 196616 | tf_op jit(solution)/shard_map/ppermute | solution.py:36

commit v2 on v1

--- a/solution.py
+++ b/solution.py
@@ -81,7 +81,7 @@
 
 
 def mixer_kernel(
-    place_ref, scale_ref, bias_ref, own_ref, theirs_ref, gain_ref, beta_ref, decay_ref, head_gain_ref,
+    place_ref, own_ref, theirs_ref, small_ref,
     query_hbm, key_hbm, value_hbm, gate_hbm, output_hbm, state_hbm,
     new_hbm, kept_ref, sent_ref, rows_ref,
     weights, output_weight, state, sems,
@@ -117,8 +117,9 @@
         pieces += ordered(own_ref, theirs_ref, chip, core)
     resid = jnp.concatenate(pieces, axis=1)
     rows_ref[...] = resid.astype(jnp.bfloat16)
-    normed_wide = rms_norm(resid, gain_ref[...])
-    normed = normed_wide.astype(jnp.bfloat16)
+    small = lambda row, size: small_ref[row : row + 1, :size]
+    vectors = 2 * heads_here
+    normed = rms_norm(resid, small_ref[vectors : vectors + 1, :]).astype(jnp.bfloat16)
     normed_wide = normed.astype(jnp.float32)
 
     def project(index):
@@ -129,14 +130,16 @@
     betas, decays = [], []
     for head in range(heads_here):
         beta_in = jnp.sum(
-            normed_wide * beta_ref[head : head + 1, :].astype(jnp.float32), axis=1, keepdims=True
+            normed_wide * small_ref[head : head + 1, :], axis=1, keepdims=True
         )
         decay_in = jnp.sum(
-            normed_wide * decay_ref[head : head + 1, :].astype(jnp.float32), axis=1, keepdims=True
-        ) + bias_ref[head]
+            normed_wide * small_ref[heads_here + head : heads_here + head + 1, :],
+            axis=1,
+            keepdims=True,
+        ) + small_ref[vectors + 3 : vectors + 4, head : head + 1]
         soft = jnp.maximum(decay_in, 0.0) + jnp.log1p(jnp.exp(-jnp.abs(decay_in)))
         betas.append(1.0 / (1.0 + jnp.exp(-beta_in)))
-        decays.append(jnp.broadcast_to(jnp.exp(-scale_ref[head] * soft), (rows_count, value_size)))
+        decays.append(jnp.broadcast_to(jnp.exp(-small_ref[vectors + 2 : vectors + 3, head : head + 1] * soft), (rows_count, value_size)))
     keys_all = project(0)
     queries_all = project(1)
     values_all = project(2)
@@ -180,7 +183,7 @@
     gated = []
     for head in heads:
         gate = cut(gates_all, head, value_size)
-        normal = rms_norm(jnp.concatenate(state_reads[head], axis=0), head_gain_ref[...])
+        normal = rms_norm(jnp.concatenate(state_reads[head], axis=0), small(vectors + 1, value_size))
         gated.append((normal * (gate / (1.0 + jnp.exp(-gate)))).astype(jnp.bfloat16))
     output_copy.wait()
     partial = jnp.dot(
@@ -191,8 +194,15 @@
         copy.wait()
 
 
-def mixer(place, own, theirs, delta_state, mix_gain, w_query, w_key, w_value, w_outgate, w_beta,
-          w_decay, decay_scale, decay_bias, head_gain, w_output):
+def pack_small(w_beta, w_decay, mix_gain, head_gain, decay_scale, decay_bias, ffn_gain):
+    columns = w_beta.shape[0]
+    row = lambda v: jnp.pad(v.astype(jnp.float32), (0, columns - v.shape[0]))[None]
+    vectors = (mix_gain, head_gain, decay_scale, decay_bias, ffn_gain)
+    rows = [w_beta.T.astype(jnp.float32), w_decay.T.astype(jnp.float32)] + [row(v) for v in vectors]
+    return jnp.concatenate(rows, axis=0)
+
+
+def mixer(place, own, theirs, small, delta_state, w_query, w_key, w_value, w_outgate, w_output):
     chips, rows_count, width = own.shape
     columns = w_query.shape[0]
     vmem = pl.BlockSpec(memory_space=pltpu.VMEM)
@@ -201,7 +211,7 @@
     return pl.pallas_call(
         mixer_kernel,
         name="mixer",
-        in_specs=[smem] * 3 + [vmem] * 6 + [hbm] * 6,
+        in_specs=[smem] + [vmem] * 3 + [hbm] * 6,
         out_specs=[hbm, vmem, vmem, vmem],
         out_shape=[
             pltpu.HBM(delta_state.shape, jnp.float32),
@@ -217,8 +227,7 @@
         ],
         compiler_params=pltpu.CompilerParams(vmem_limit_bytes=40 * 2**20),
     )(
-        place, decay_scale, decay_bias, own, theirs, mix_gain[None], w_beta.T, w_decay.T,
-        head_gain[None],
+        place, own, theirs, small,
         *[pltpu.with_memory_space_constraint(array, pltpu.HBM)
           for array in (w_query, w_key, w_value, w_outgate, w_output, delta_state)],
     )
@@ -233,7 +242,7 @@
     for chip in range(chips):
         pieces += ordered(own_ref, theirs_ref, chip, core)
     resid = jnp.concatenate(pieces, axis=1) + rows_ref[...].astype(jnp.float32)
-    normed = rms_norm(resid, gain_ref[...]).astype(jnp.bfloat16)
+    normed = rms_norm(resid, gain_ref[gain_ref.shape[0] - 1 :, :]).astype(jnp.bfloat16)
     normed_ref[...] = normed
     outgoing = jnp.dot(choose_ref[...], normed, preferred_element_type=jnp.float32)
     outgoing_ref[...] = outgoing.astype(jnp.bfloat16)
@@ -256,7 +265,7 @@
             jax.ShapeDtypeStruct(rows.shape, jnp.bfloat16),
             jax.ShapeDtypeStruct(own.shape[1:], jnp.float32),
         ],
-    )(place, own, theirs, rows, gain[None], choose)
+    )(place, own, theirs, rows, gain, choose)
 
 
 def body(
@@ -289,10 +298,11 @@
     core = tp_index % 2
     place = tp_index[None]
     chips = lax.axis_size("tp") // 2
+    small = pack_small(w_beta, w_decay, mix_gain, head_gain, decay_scale, decay_bias, ffn_gain)
     own_rows = exchange_chips(jnp.broadcast_to(tokens[None], (chips,) + tokens.shape))
     new_state, kept, sent, full_rows = mixer(
-        place, own_rows, swap_cores(own_rows), delta_state, mix_gain, w_query, w_key, w_value,
-        w_outgate, w_beta, w_decay, decay_scale, decay_bias, head_gain, w_output,
+        place, own_rows, swap_cores(own_rows), small, delta_state, w_query, w_key, w_value,
+        w_outgate, w_output,
     )
     halves = (kept + swap_cores(sent).astype(jnp.float32)).astype(jnp.bfloat16)
     mixed = sum_chips(halves)
@@ -320,7 +330,7 @@
     )
     by_row = jnp.sum(choose.reshape(rows_count, top_count, slot_count), axis=1)
     outgoing, normed_ffn, resid_own = dispatch(
-        place, mixed, swap_cores(mixed), full_rows, ffn_gain, by_row.T
+        place, mixed, swap_cores(mixed), full_rows, small, by_row.T
     )
     outgoing = outgoing.reshape(ep_count, experts_here, capacity, model_width)
     results = expert_block(

time: 81.4 us -> 77.6 us (0.953)
  waiting for transfers between devices: 26.3 us -> 22.7 us
  local copies, waits for them, and re-layouts: 10.4 us -> 7.2 us
  other arithmetic: 1.16 us -> 3.93 us
    unnamed x34 -> x24, local copies, waits for them, and re-layouts: 5.53 us -> 2.19 us
    all_to_all x2, waiting for transfers between devices: 13.3 us -> 10.1 us  [exchange_chips(): lax.all_to_all(blocks, 'tp', 0, 0, tiled=True, axis_index_groups=chip_gro...]
    broadcast_in_dim x0 -> x3, other arithmetic: none -> 2.04 us  [pack_small(): jnp.pad(v.astype(jnp.float32), (0, columns - v.shape[0]))[None]]
    pad x0 -> x2, local copies, waits for them, and re-layouts: none -> 1.32 us  [pack_small(): jnp.pad(v.astype(jnp.float32), (0, columns - v.shape[0]))[None]]
    broadcast_in_dim x2 -> x0, local copies, waits for them, and re-layouts: 1.29 us -> none  [the longest x1 0.69 us: mixer(): mix_gain[None]]
  transfers between devices with their start and end apart: 8 -> 8, of which waited for: 7 -> 8; matrix products, arithmetic and copies ran while one was open for 6% -> 10% of each run, Pallas kernels for 0% -> 0%
where the time goes in v2:
time: 77.6 us; the launch traced here: 76.8 us
  waiting for transfers between devices  22.7 us (29%)
  starting transfers between devices  17.9 us (23%)
  Pallas kernels  8.82 us (11%)
  blocking collectives  8.24 us (11%)
  local copies, waits for them, and re-layouts  7.2 us (9%)
  matrix products  7.08 us (9%)
  other arithmetic  3.93 us (5%)
  between operations  0.9 us (1%)
    all_to_all x2, starting transfers between devices, exchange_chips(): lax.all_to_all(blocks, 'tp', 0, 0, tiled=True, axis_index_groups=chip_gro...  10.4 us
    all_to_all x2, waiting for transfers between devices, exchange_chips(): lax.all_to_all(blocks, 'tp', 0, 0, tiled=True, axis_index_groups=chip_gro...  10.1 us
    all_to_all x1, blocking collectives, exchange_chips(): lax.all_to_all(blocks, 'tp', 0, 0, tiled=True, axis_index_groups=chip_gro...  8.24 us
    pallas_call x1, Pallas kernels, mixer(): pl.pallas_call(mixer_kernel, name='mixer', in_specs=[smem] + [vmem] * 3 +...  6.71 us
    all_to_all x1, waiting for transfers between devices, body(): lax.all_to_all(results, 'ep', split_axis=0, concat_axis=0, tiled=True)  4.9 us
    all_to_all x1, waiting for transfers between devices, body(): lax.all_to_all(outgoing, 'ep', split_axis=0, concat_axis=0, tiled=True)  4.59 us
    all_to_all x1, starting transfers between devices, body(): lax.all_to_all(outgoing, 'ep', split_axis=0, concat_axis=0, tiled=True)  3.72 us
    all_to_all x1, starting transfers between devices, body(): lax.all_to_all(results, 'ep', split_axis=0, concat_axis=0, tiled=True)  3.54 us
  transfers between devices with their start and end apart: 8, of which 8 were waited for; matrix products, arithmetic and copies ran while one was open for 10% of the time, Pallas kernels for 0%

profile of v2, /device:TPU:0, one launch (start us, length us, event | category | flops | bytes accessed | tf_op | source)
XLA Modules:
  0.0 76.8 jit_solution(10802483757556806801)
XLA Ops:
  0.6 0.0 copy-start
  0.6 1.5 %broadcast_in_dim.63 = bf16[4,32,256]{2,1,0:T(8,128)(2,1)} broadcast(bf16[32,256]{1,0:T(8,128)(2,1)} %param.22), dimensions={1,2} | broadcast | bytes 81920 | tf_op jit(solution)/shard_map/broadcast_in_dim | solution.py:302
  2.1 6.3 %all-to-all-start = ((bf16[4,32,256]{2,1,0:T(8,128)(2,1)}), bf16[4,32,256]{2,1,0:T(8,128)(2,1)S(1)}, u32[]{:S(2)}, u32[]{:S(2)}) async-start(bf16[4,32,256]{2,1,0:T(8,128)(2,1)} %broadcast_in_dim.63), calls=%async_computation | async-start | bytes 131072 | tf_op jit(solution)/shard_map/all_to_all | solution.py:30
  8.5 0.7 broadcast_in_dim.76
  9.2 0.7 pad.13
  9.8 0.7 pad.14
  10.5 0.7 broadcast_in_dim.78
  11.2 0.8 copy.46
  12.0 0.1 eq.54
  12.1 0.7 convert_bitcast_fusion
  12.8 0.2 convert_reduce_fusion
  13.0 0.1 reduce_sum.55
  13.1 1.1 %all-to-all-done.own_ref = bf16[4,32,256]{2,1,0:T(8,128)(2,1)S(1)} async-done(((bf16[4,32,256]{2,1,0:T(8,128)(2,1)}), bf16[4,32,256]{2,1,0:T(8,128)(2,1)S(1)}, u32[]{:S(2)}, u32[]{:S(2)}) %all-to-all-start) | async-done | bytes 65568 | tf_op jit(solution)/shard_map/all_to_all | solution.py:30
  14.2 0.0 collective-permute-start
  14.2 0.7 pad_convert_fusion
  14.9 0.1 concatenate.9.small_ref.gain_ref
  15.0 0.0 copy-start.1
  15.0 0.5 collective-permute-done.theirs_ref
  15.5 6.7 %mixer.1 = (f32[32,2,128,128]{3,2,1,0:T(8,128)}, f32[4,32,256]{2,1,0:T(8,128)S(1)}, bf16[4,32,256]{2,1,0:T(8,128)(2,1)S(1)}, bf16[32,2048]{1,0:T(8,128)(2,1)S(1)}) custom-call(s32[1]{0:T(128)} %bitcast.place_ref, bf16[4,32,256]{2,1,0:T(8,128)(2,1)S(1)} %all-to-all-done.own_ref, bf16[4,32,256]{2,1,0:T(8,128)(2,1)S(1)} %collective-permute-done.theirs_ref, ...), custom_call_target="tpu_custom_call" | custom-call | tf_op jit(solution)/shard_map/mixer/pallas_call | solution.py:211
  22.2 0.0 copy-done.1
  22.2 0.0 copy-start.2
  22.2 0.7 copy-done.2
  22.9 0.2 collective-permute-start.1
  23.1 0.0 copy-done.10
  23.1 0.1 copy.53
  23.2 1.0 %collective-permute-done.1 = bf16[4,32,256]{2,1,0:T(8,128)(2,1)S(1)} collective-permute-done((bf16[4,32,256]{2,1,0:T(8,128)(2,1)S(1)}, bf16[4,32,256]{2,1,0:T(8,128)(2,1)S(1)}, u32[]{:S(2)}, u32[]{:S(2)}) %collective-permute-start.1) | collective-permute-done | bytes 65568 | tf_op jit(solution)/shard_map/ppermute | solution.py:36
  24.2 0.7 broadcast_in_dim.72
  24.9 4.0 %all-to-all-start.1 = ((bf16[16,32,256]{2,1,0:T(8,128)(2,1)}), bf16[16,32,256]{2,1,0:T(8,128)(2,1)S(1)}, u32[]{:S(2)}, u32[]{:S(2)}) async-start(bf16[16,32,256]{2,1,0:T(8,128)(2,1)} %bitcast.8), calls=%async_computation.1 | async-start | bytes 524288 | tf_op jit(solution)/shard_map/all_to_all | solution.py:30
  28.9 0.1 copy.51
  29.0 0.1 copy.54
  29.1 0.1 select_reduce_fusion
  29.2 8.9 %all-to-all-done.1 = bf16[16,32,256]{2,1,0:T(8,128)(2,1)S(1)} async-done(((bf16[16,32,256]{2,1,0:T(8,128)(2,1)}), bf16[16,32,256]{2,1,0:T(8,128)(2,1)S(1)}, u32[]{:S(2)}, u32[]{:S(2)}) %all-to-all-start.1) | async-done | bytes 262176 | tf_op jit(solution)/shard_map/all_to_all | solution.py:30
  38.2 0.0 copy-start.6
  38.2 0.1 collective-permute-start.2
  38.3 0.1 fusion.37
  38.4 0.7 copy.52
  39.1 0.4 collective-permute-done.2.theirs_ref
  39.5 0.0 copy-done.6
  39.5 0.6 copy-done.8
  40.2 2.1 %dispatch.1 = (bf16[64,2048]{1,0:T(8,128)(2,1)}, bf16[32,2048]{1,0:T(8,128)(2,1)}, f32[32,256]{1,0:T(8,128)}) custom-call(s32[1]{0:T(128)} %bitcast.place_ref, bf16[4,32,256]{2,1,0:T(8,128)(2,1)} %copy-done.6, bf16[4,32,256]{2,1,0:T(8,128)(2,1)} %copy-done.8, bf16[32,2048]{1,0:T(8,128)(2,1)} %copy-done.2, f32[9,2048]{1,0:T(8,128)} %copy-done.1, ...), custom_call_target="tpu_custom_call" | custom-call | tf_op jit(solution)/shard_map/dispatch/pallas_call | solution.py:258
  42.3 3.7 %all-to-all-start.2 = ((bf16[4,1,16,2048]{3,2,1,0:T(8,128)(2,1)}), bf16[4,1,16,2048]{3,2,1,0:T(8,128)(2,1)S(1)}, u32[]{:S(2)}, u32[]{:S(2)}) async-start(bf16[4,1,16,2048]{3,2,1,0:T(8,128)(2,1)} %bitcast.97), calls=%async_computation.2 | async-start | bytes 524288 | tf_op jit(solution)/shard_map/all_to_all | solution.py:337
  46.0 0.0 copy-done.7
  46.0 1.1 %fusion.56 = f32[32,64]{1,0:T(8,128)S(1)} fusion(bf16[32,2048]{1,0:T(8,128)(2,1)} %get-tuple-element.14, bf16[2048,64]{0,1:T(8,128)(2,1)S(1)} %copy-done.7), kind=kOutput, calls=%fused_computation.66 | convolution fusion | flops 8388608 | bytes 401408 | tf_op jit(solution)/shard_map/dot_general | solution.py:355
  47.1 4.6 %all-to-all-done.2 = bf16[4,1,16,2048]{3,2,1,0:T(8,128)(2,1)S(1)} async-done(((bf16[4,1,16,2048]{3,2,1,0:T(8,128)(2,1)}), bf16[4,1,16,2048]{3,2,1,0:T(8,128)(2,1)S(1)}, u32[]{:S(2)}, u32[]{:S(2)}) %all-to-all-start.2) | async-done | bytes 262176 | tf_op jit(solution)/shard_map/all_to_all | solution.py:337
  51.7 2.1 %fusion.6 = f32[4,1,16,512]{3,2,0,1:T(8,128)S(1)} fusion(bf16[1,2048,512]{2,1,0:T(8,128)(2,1)} %param.38, bf16[4,1,16,2048]{3,2,1,0:T(8,128)(2,1)S(1)} %all-to-all-done.2), kind=kOutput, calls=%fused_computation.8 | convolution fusion | flops 134217728 | bytes 2490368 | tf_op jit(solution)/shard_map/sjnd,jdf->sjnf/dot_general | solution.py:62
  53.7 0.0 copy-done
  53.7 0.0 copy-start.3
  53.7 0.0 copy-start.4
  53.8 0.0 copy-start.5
  53.8 3.3 %fusion = bf16[4,1,16,2048]{3,2,1,0:T(8,128)(2,1)} fusion(bf16[1,512,2048]{2,1,0:T(8,128)(2,1)S(1)} %copy-done, bf16[1,2048,512]{2,1,0:T(8,128)(2,1)} %param.39, bf16[4,1,16,2048]{3,2,1,0:T(8,128)(2,1)S(1)} %all-to-all-done.2, f32[4,1,16,512]{3,2,0,1:T(8,128)S(1)} %fusion.6), kind=kOutput, calls=%fused_computation.1 | convolution fusion | flops 268763136 | bytes 4849664 | tf_op jit(solution)/shard_map/sjnf,jfd->sjnd/dot_general | solution.py:65
  57.0 3.5 %all-to-all-start.3 = ((bf16[4,1,16,2048]{3,2,1,0:T(8,128)(2,1)}), bf16[4,1,16,2048]{3,2,1,0:T(8,128)(2,1)S(1)}, u32[]{:S(2)}, u32[]{:S(2)}) async-start(bf16[4,1,16,2048]{3,2,1,0:T(8,128)(2,1)} %fusion), calls=%async_computation.3 | async-start | bytes 524288 | tf_op jit(solution)/shard_map/all_to_all | solution.py:342
  60.6 0.0 copy-done.3
  60.6 0.0 copy-done.4
  60.6 0.0 copy-done.5
  60.6 0.4 fusion.46
  61.0 4.9 %all-to-all-done.3 = bf16[4,1,16,2048]{3,2,1,0:T(8,128)(2,1)S(1)} async-done(((bf16[4,1,16,2048]{3,2,1,0:T(8,128)(2,1)}), bf16[4,1,16,2048]{3,2,1,0:T(8,128)(2,1)S(1)}, u32[]{:S(2)}, u32[]{:S(2)}) %all-to-all-start.3) | async-done | bytes 262176 | tf_op jit(solution)/shard_map/all_to_all | solution.py:342
  65.9 0.3 convolution_add_fusion
  66.2 0.2 reshape.140
  66.4 0.1 copy.59
  66.5 0.1 collective-permute-start.3
  66.6 1.2 %collective-permute-done.3 = bf16[4,32,256]{2,1,0:T(8,128)(2,1)S(1)} collective-permute-done((bf16[4,32,256]{2,1,0:T(8,128)(2,1)S(1)}, bf16[4,32,256]{2,1,0:T(8,128)(2,1)S(1)}, u32[]{:S(2)}, u32[]{:S(2)}) %collective-permute-start.3) | collective-permute-done | bytes 65568 | tf_op jit(solution)/shard_map/ppermute | solution.py:36
  67.9 8.2 %all_to_all.25 = bf16[4,32,256]{2,1,0:T(8,128)(2,1)S(1)} all-to-all(bf16[4,32,256]{2,1,0:T(8,128)(2,1)S(1)} %fusion.30), channel_id=1, replica_groups={{0,2,4,6},{1,3,5,7},{8,10,12,14},{9,11,13,15},{16,18,20,22},{17,19,21,2..., dimensions={0} | all-to-all | bytes 131072 | tf_op jit(solution)/shard_map/all_to_all | solution.py:30
  76.1 0.0 copy-done.9
  76.2 0.6 add_convert_fusion.1
  (12 shorter events, 0.2 us)
Async XLA Ops:
  0.6 53.1 %copy-start = (bf16[1,512,2048]{2,1,0:T(8,128)(2,1)S(1)}, bf16[1,512,2048]{2,1,0:T(8,128)(2,1)}, u32[]{:S(2)}) copy-start(bf16[1,512,2048]{2,1,0:T(8,128)(2,1)} %param.40) | copy-start | bytes 6291460
  2.1 12.1 %all-to-all-start = ((bf16[4,32,256]{2,1,0:T(8,128)(2,1)}), bf16[4,32,256]{2,1,0:T(8,128)(2,1)S(1)}, u32[]{:S(2)}, u32[]{:S(2)}) async-start(bf16[4,32,256]{2,1,0:T(8,128)(2,1)} %broadcast_in_dim.63), calls=%async_computation | async-start | bytes 131072 | tf_op jit(solution)/shard_map/all_to_all | solution.py:30
  14.2 1.3 %collective-permute-start = (bf16[4,32,256]{2,1,0:T(8,128)(2,1)S(1)}, bf16[4,32,256]{2,1,0:T(8,128)(2,1)S(1)}, u32[]{:S(2)}, u32[]{:S(2)}) collective-permute-start(bf16[4,32,256]{2,1,0:T(8,128)(2,1)S(1)} %all-to-all-done.own_ref), channel_id=1, source_target_pairs={{0,1},{1,0},{2,3},{3,2},{4,5},{5,4},{6,7},{7,6},{8,9},{9,8},{10,11... | collective-permute-start | bytes 196616 | tf_op jit(solution)/shard_map/ppermute | solution.py:36
  15.0 7.2 %copy-start.1 = (f32[9,2048]{1,0:T(8,128)}, f32[9,2048]{1,0:T(8,128)S(1)}, u32[]{:S(2)}) copy-start(f32[9,2048]{1,0:T(8,128)S(1)} %concatenate.9.small_ref.gain_ref) | copy-start | bytes 221188
  15.5 7.6 %copy-start.10 = (f32[32,6]{0,1:T(8,128)S(1)}, f32[32,6]{0,1:T(8,128)}, u32[]{:S(2)}) copy-start(f32[32,6]{0,1:T(8,128)} %param.37) | copy-start | bytes 2308
  22.2 0.7 copy-start.2
  22.9 23.1 %copy-start.7 = (bf16[2048,64]{0,1:T(8,128)(2,1)S(1)}, bf16[2048,64]{0,1:T(8,128)(2,1)}, u32[]{:S(2)}) copy-start(bf16[2048,64]{0,1:T(8,128)(2,1)} %param.41) | copy-start | bytes 786436
  22.9 1.3 %collective-permute-start.1 = (bf16[4,32,256]{2,1,0:T(8,128)(2,1)S(1)}, bf16[4,32,256]{2,1,0:T(8,128)(2,1)S(1)}, u32[]{:S(2)}, u32[]{:S(2)}) collective-permute-start(bf16[4,32,256]{2,1,0:T(8,128)(2,1)S(1)} %get-tuple-element.10), channel_id=1, source_target_pairs={{0,1},{1,0},{2,3},{3,2},{4,5},{5,4},{6,7},{7,6},{8,9},{9,8},{10,11... | collective-permute-start | bytes 196616 | tf_op jit(solution)/shard_map/ppermute | solution.py:36
  24.9 13.3 %all-to-all-start.1 = ((bf16[16,32,256]{2,1,0:T(8,128)(2,1)}), bf16[16,32,256]{2,1,0:T(8,128)(2,1)S(1)}, u32[]{:S(2)}, u32[]{:S(2)}) async-start(bf16[16,32,256]{2,1,0:T(8,128)(2,1)} %bitcast.8), calls=%async_computation.1 | async-start | bytes 524288 | tf_op jit(solution)/shard_map/all_to_all | solution.py:30
  38.2 1.3 %copy-start.6 = (bf16[4,32,256]{2,1,0:T(8,128)(2,1)}, bf16[4,32,256]{2,1,0:T(8,128)(2,1)S(1)}, u32[]{:S(2)}) copy-start(bf16[4,32,256]{2,1,0:T(8,128)(2,1)S(1)} %reduce_sum.53.own_ref) | copy-start | bytes 196612
  38.2 1.3 %collective-permute-start.2 = (bf16[4,32,256]{2,1,0:T(8,128)(2,1)S(1)}, bf16[4,32,256]{2,1,0:T(8,128)(2,1)S(1)}, u32[]{:S(2)}, u32[]{:S(2)}) collective-permute-start(bf16[4,32,256]{2,1,0:T(8,128)(2,1)S(1)} %reduce_sum.53.own_ref), channel_id=1, source_target_pairs={{0,1},{1,0},{2,3},{3,2},{4,5},{5,4},{6,7},{7,6},{8,9},{9,8},{10,11... | collective-permute-start | bytes 196616 | tf_op jit(solution)/shard_map/ppermute | solution.py:36
  39.5 0.6 copy-start.8
  42.3 9.4 %all-to-all-start.2 = ((bf16[4,1,16,2048]{3,2,1,0:T(8,128)(2,1)}), bf16[4,1,16,2048]{3,2,1,0:T(8,128)(2,1)S(1)}, u32[]{:S(2)}, u32[]{:S(2)}) async-start(bf16[4,1,16,2048]{3,2,1,0:T(8,128)(2,1)} %bitcast.97), calls=%async_computation.2 | async-start | bytes 524288 | tf_op jit(solution)/shard_map/all_to_all | solution.py:337
  53.7 6.9 %copy-start.3 = (bf16[32,2048]{1,0:T(8,128)(2,1)S(1)}, bf16[32,2048]{1,0:T(8,128)(2,1)}, u32[]{:S(2)}) copy-start(bf16[32,2048]{1,0:T(8,128)(2,1)} %get-tuple-element.14) | copy-start | bytes 393220
  53.7 6.9 %copy-start.4 = (bf16[64,2048]{1,0:T(8,128)(2,1)S(1)}, bf16[64,2048]{1,0:T(8,128)(2,1)}, u32[]{:S(2)}) copy-start(bf16[64,2048]{1,0:T(8,128)(2,1)} %param.43) | copy-start | bytes 786436
  53.8 6.9 %copy-start.5 = (bf16[2048,64]{0,1:T(8,128)(2,1)S(1)}, bf16[2048,64]{0,1:T(8,128)(2,1)}, u32[]{:S(2)}) copy-start(bf16[2048,64]{0,1:T(8,128)(2,1)} %param.42) | copy-start | bytes 786436
  57.0 19.1 %copy-start.9 = (f32[32,256]{1,0:T(8,128)S(1)}, f32[32,256]{1,0:T(8,128)}, u32[]{:S(2)}) copy-start(f32[32,256]{1,0:T(8,128)} %get-tuple-element.12) | copy-start | bytes 98308
  57.0 8.9 %all-to-all-start.3 = ((bf16[4,1,16,2048]{3,2,1,0:T(8,128)(2,1)}), bf16[4,1,16,2048]{3,2,1,0:T(8,128)(2,1)S(1)}, u32[]{:S(2)}, u32[]{:S(2)}) async-start(bf16[4,1,16,2048]{3,2,1,0:T(8,128)(2,1)} %fusion), calls=%async_computation.3 | async-start | bytes 524288 | tf_op jit(solution)/shard_map/all_to_all | solution.py:342
  66.5 1.3 %collective-permute-start.3 = (bf16[4,32,256]{2,1,0:T(8,128)(2,1)S(1)}, bf16[4,32,256]{2,1,0:T(8,128)(2,1)S(1)}, u32[]{:S(2)}, u32[]{:S(2)}) collective-permute-start(bf16[4,32,256]{2,1,0:T(8,128)(2,1)S(1)} %fusion.38), channel_id=1, source_target_pairs={{0,1},{1,0},{2,3},{3,2},{4,5},{5,4},{6,7},{7,6},{8,9},{9,8},{10,11... | collective-permute-start | bytes 196616 | tf_op jit(solution)/shard_map/ppermute | solution.py:36
